TPU v7x, 32 devices: a whole 2x2x4 slice. The times are simulated.
32 devices in a mesh: ep: 16 (over z, y, x), tp: 2 (over core).
Axes of the slice: x: 2, y: 2, z: 4, core: 2. Of those that a mesh axis runs over, the one named last changes fastest.
Arguments:
- tokens: bfloat16 [256, 2048], P('ep'), may hold values from -6 to 6
- state: float32 [256, 8, 128, 128], P('ep', 'tp'), may hold values from -6 to 6
- mix_gain: float32 [2048], replicated, may hold values from 0.1 to 1.9
- moe_gain: float32 [2048], replicated, may hold values from 0.1 to 1.9
- head_gain: float32 [128], replicated, may hold values from 0.1 to 1.9
- w_forget: bfloat16 [2048, 1024], P(None, 'tp'), may hold values from -0.125 to 0.125
- w_query: bfloat16 [2048, 1024], P(None, 'tp'), may hold values from -0.125 to 0.125
- w_input: bfloat16 [2048, 1024], P(None, 'tp'), may hold values from -0.125 to 0.125
- w_outgate: bfloat16 [2048, 1024], P(None, 'tp'), may hold values from -0.125 to 0.125
- lower_bound: float32 [1024], P('tp'), may hold values from 0 to 0.9
- w_mix_out: bfloat16 [1024, 2048], P('tp'), may hold values from -0.1875 to 0.1875
- routes: int32 [256, 6], P('ep'), may hold values from 0 to 15, all different within a row; in each aligned block of 16 rows (0 to 15, 16 to 31, ...) at most 16 rows name the same one
- route_scores: float32 [256, 6], P('ep'), may hold values from 0.05 to 1
- expert_gate: bfloat16 [16, 2048, 512], P('ep', None, 'tp'), may hold values from -0.125 to 0.125
- expert_up: bfloat16 [16, 2048, 512], P('ep', None, 'tp'), may hold values from -0.125 to 0.125
- expert_down: bfloat16 [16, 512, 2048], P('ep', 'tp'), may hold values from -0.25 to 0.25
- shared_gate: bfloat16 [2048, 512], P(None, 'tp'), may hold values from -0.125 to 0.125
- shared_up: bfloat16 [2048, 512], P(None, 'tp'), may hold values from -0.125 to 0.125
- shared_down: bfloat16 [512, 2048], P('tp'), may hold values from -0.25 to 0.25
Outputs:
- layer_out: bfloat16 [256, 2048], P('ep', 'tp')
- new_state: float32 [256, 8, 128, 128], P('ep', 'tp')
Inputs may be any that keep to these rules, and one draw needn't show every extreme that they name: `routes`: each token names 6 different experts. Among the tokens of one index of ep no expert is named by more than 16 tokens, and in every draw some expert is named by exactly 16 tokens of some index of ep.
All inputs are finite; a program needn't handle non-finite values.
Results may differ from a plain program's by a relative error of at most 0.017.
Values may be sent and summed in bfloat16 or wider, within the bound.
No kernel may reach another device: no remote copies, remote signals or barrier semaphores. Data moves between devices by JAX's collectives and lax.ppermute only.
A program may use at most 128 MiB of HBM per device.

v0:
```python
import jax
import jax.numpy as jnp
from jax import lax
from jax.sharding import PartitionSpec as P

epsilon = 1e-06
routed_scale = 2.5


def rms_scale(values, gain):
    return values * lax.rsqrt(jnp.mean(values * values, axis=-1, keepdims=True) + epsilon) * gain


def local(
    tokens,
    state,
    mix_gain,
    moe_gain,
    head_gain,
    w_forget,
    w_query,
    w_input,
    w_outgate,
    lower_bound,
    w_mix_out,
    routes,
    route_scores,
    expert_gate,
    expert_up,
    expert_down,
    shared_gate,
    shared_up,
    shared_down,
):
    seqs_here = tokens.shape[0]
    heads_here = state.shape[1]
    key_width = state.shape[2]
    value_width = state.shape[3]
    tokens_wide = tokens.astype(jnp.float32)
    normed = rms_scale(tokens_wide, mix_gain).astype(jnp.bfloat16)
    forget_pre = jnp.dot(normed, w_forget, preferred_element_type=jnp.float32).reshape(
        seqs_here, heads_here, key_width
    )
    query = jax.nn.silu(jnp.dot(normed, w_query, preferred_element_type=jnp.float32)).reshape(
        seqs_here, heads_here, key_width
    )
    input_val = jnp.dot(normed, w_input, preferred_element_type=jnp.float32).reshape(
        seqs_here, heads_here, value_width
    )
    gate_pre = jnp.dot(normed, w_outgate, preferred_element_type=jnp.float32).reshape(
        seqs_here, heads_here, value_width
    )
    bound_rows = lower_bound.reshape(heads_here, key_width)
    forget = bound_rows + (1.0 - bound_rows) * jax.nn.sigmoid(forget_pre)
    key_gate = (1.0 - bound_rows) * jax.nn.sigmoid(-forget_pre)
    new_state = forget[..., None] * state + key_gate[..., None] * input_val[:, :, None, :]
    readout = jnp.einsum("shkv,shk->shv", new_state, query, precision=lax.Precision.HIGHEST)
    gated_out = (rms_scale(readout, head_gain) * jax.nn.silu(gate_pre)).astype(jnp.bfloat16)
    gated_out = gated_out.reshape(seqs_here, heads_here * value_width)
    partial_value = jnp.dot(gated_out, w_mix_out, preferred_element_type=jnp.float32)
    mixer_out = lax.psum(partial_value.astype(jnp.bfloat16), "tp")
    residual = tokens_wide + mixer_out.astype(jnp.float32)
    moe_rows = rms_scale(residual, moe_gain).astype(jnp.bfloat16)
    full_width = moe_rows.shape[1]
    half_width = full_width // 2
    tp_index = lax.axis_index("tp")
    shared_hidden = (
        jax.nn.silu(jnp.dot(moe_rows, shared_gate, preferred_element_type=jnp.float32))
        * jnp.dot(moe_rows, shared_up, preferred_element_type=jnp.float32)
    ).astype(jnp.bfloat16)
    shared_part = jnp.dot(shared_hidden, shared_down, preferred_element_type=jnp.float32)
    shared_out = lax.psum_scatter(
        shared_part.astype(jnp.bfloat16), "tp", scatter_dimension=1, tiled=True
    )
    top_count = routes.shape[1]
    experts_all = expert_gate.shape[0] * lax.axis_size("ep")
    capacity = max(2, min(seqs_here, seqs_here * top_count * 3 // experts_all))
    flat_routes = routes.reshape(-1)
    onehot = (flat_routes[:, None] == jnp.arange(experts_all, dtype=jnp.int32)[None, :]).astype(
        jnp.int32
    )
    earlier = jnp.cumsum(onehot, axis=0) - onehot
    slot_rank = jnp.sum(earlier * onehot, axis=1)
    slot_index = flat_routes * capacity + slot_rank
    placing = (
        slot_index[None, :] == jnp.arange(experts_all * capacity, dtype=jnp.int32)[:, None]
    ).astype(jnp.int32)
    placing = (
        placing.reshape(experts_all * capacity, seqs_here, top_count)
        .sum(axis=2)
        .astype(jnp.bfloat16)
    )
    own_columns = lax.dynamic_slice_in_dim(moe_rows, tp_index * half_width, half_width, 1)
    outgoing = jnp.dot(placing, own_columns, preferred_element_type=jnp.float32).astype(
        jnp.bfloat16
    )
    outgoing = outgoing.reshape(experts_all, capacity, half_width)
    arrived_half = lax.all_to_all(outgoing, "ep", split_axis=0, concat_axis=1, tiled=True)
    arrived = lax.all_gather(arrived_half, "tp", axis=2, tiled=True)
    gate_act = jnp.einsum("esd,edf->esf", arrived, expert_gate, preferred_element_type=jnp.float32)
    up_act = jnp.einsum("esd,edf->esf", arrived, expert_up, preferred_element_type=jnp.float32)
    expert_hidden = (jax.nn.silu(gate_act) * up_act).astype(jnp.bfloat16)
    expert_part = jnp.einsum(
        "esf,efd->esd", expert_hidden, expert_down, preferred_element_type=jnp.float32
    )
    expert_half = lax.psum_scatter(
        expert_part.astype(jnp.bfloat16), "tp", scatter_dimension=2, tiled=True
    )
    returned = lax.all_to_all(expert_half, "ep", split_axis=1, concat_axis=0, tiled=True)
    pair_out = returned.reshape(experts_all * capacity, half_width)[slot_index].astype(jnp.float32)
    weights = route_scores / jnp.sum(route_scores, axis=-1, keepdims=True) * routed_scale
    routed = jnp.sum(
        pair_out.reshape(seqs_here, top_count, half_width) * weights[:, :, None], axis=1
    )
    residual_half = lax.dynamic_slice_in_dim(residual, tp_index * half_width, half_width, 1)
    layer_out = (residual_half + routed + shared_out.astype(jnp.float32)).astype(jnp.bfloat16)
    return (layer_out, new_state)


def solution(mesh):
    return jax.shard_map(
        local,
        mesh=mesh,
        in_specs=(
            P("ep", None),
            P("ep", "tp", None, None),
            P(),
            P(),
            P(),
            P(None, "tp"),
            P(None, "tp"),
            P(None, "tp"),
            P(None, "tp"),
            P("tp"),
            P("tp", None),
            P("ep", None),
            P("ep", None),
            P("ep", None, "tp"),
            P("ep", None, "tp"),
            P("ep", "tp", None),
            P(None, "tp"),
            P(None, "tp"),
            P("tp", None),
        ),
        out_specs=(P("ep", "tp"), P("ep", "tp", None, None)),
        check_vma=False,
    )
```

profile of v0, /device:TPU:0, one launch (start us, length us, event | category | flops | bytes accessed | tf_op | source)
XLA Modules:
  0.0 138.7 jit_solution(9879463072840509546)
XLA Ops:
  7.2 0.0 all-reduce.2.cloned.1.call-start
  7.2 1.1 fusion.18
  8.4 2.1 %fusion.40 = f32[16,512]{1,0:T(8,128)S(1)} fusion(bf16[2048,512]{1,0:T(8,128)(2,1)} %param.27, bf16[16,2048]{1,0:T(8,128)(2,1)} %param.19, f32[2048]{0:T(1024)} %param.21, f32[16]{0:T(128)S(1)} %add_rsqrt_fusion.2), kind=kOutput, calls=%fused_computation.72 | convolution fusion | flops 33685504 | bytes 2203712 | tf_op jit(solution)/shard_map/dot_general | solution.py:50
  10.5 2.0 %fusion.44 = f32[16,512]{1,0:T(8,128)S(1)} fusion(bf16[2048,512]{1,0:T(8,128)(2,1)} %param.26, bf16[16,2048]{1,0:T(8,128)(2,1)S(1)} %copy-done.3, f32[2048]{0:T(1024)S(1)} %copy-done.5, f32[16]{0:T(128)S(1)} %add_rsqrt_fusion.2), kind=kOutput, calls=%fused_computation.74 | convolution fusion | flops 33685504 | bytes 2203712 | tf_op jit(solution)/shard_map/dot_general | solution.py:47
  12.5 2.0 %add_divide_fusion.1 = (f32[16,512]{1,0:T(8,128)S(1)}, f32[16,512]{1,0:T(8,128)S(1)}) fusion(bf16[2048,512]{1,0:T(8,128)(2,1)} %param.24, bf16[16,2048]{1,0:T(8,128)(2,1)S(1)} %copy-done.3, f32[2048]{0:T(1024)S(1)} %copy-done.5, f32[16]{0:T(128)S(1)} %add_rsqrt_fusion.2), kind=kOutput, calls=%fused_computation.46 | convolution fusion | flops 33726464 | bytes 2236480 | tf_op jit(solution)/shard_map/dot_general | solution.py:41
  14.6 2.0 %divide_multiply_fusion.1 = f32[16,512]{1,0:T(8,128)S(1)} fusion(bf16[2048,512]{1,0:T(8,128)(2,1)} %param.25, bf16[16,2048]{1,0:T(8,128)(2,1)S(1)} %copy-done.3, f32[2048]{0:T(1024)S(1)} %copy-done.5, f32[16]{0:T(128)S(1)} %add_rsqrt_fusion.2), kind=kOutput, calls=%fused_computation.43 | convolution fusion | flops 33718272 | bytes 2203712 | tf_op jit(solution)/shard_map/dot_general | solution.py:44
  16.7 4.4 %multiply_add_fusion = f32[16,4,128,128]{3,2,1,0:T(8,128)S(1)} fusion(f32[16,4,128,128]{3,2,1,0:T(8,128)} %param.20, f32[16,4,128]{2,1,0:T(4,128)S(1)} %mul.181, f32[16,4,128]{2,1,0:T(4,128)S(1)} %bitcast.70, f32[16,4,128]{2,1,0:T(4,128)S(1)} %bitcast.69), kind=kLoop, calls=%fused_computation.1 | loop fusion | flops 3145728 | bytes 8486912 | tf_op jit(solution)/shard_map/add | solution.py:56
  21.2 3.7 %fusion.50 = f32[16,4,1,128]{3,2,1,0:T(1,128)S(1)} fusion(f32[16,4,128,128]{3,2,1,0:T(8,128)S(1)} %multiply_add_fusion, f32[16,4,128,1]{2,3,1,0:T(1,128)S(1)} %bitcast.71), kind=kOutput, calls=%fused_computation.77 | convolution fusion | flops 12582912 | bytes 4259840 | tf_op jit(solution)/shard_map/shkv,shk->shv/dot_general | solution.py:57
  24.8 0.1 multiply_reduce_fusion.2
  25.0 0.1 fusion.25
  25.1 1.0 convolution_convert_fusion.2
  26.1 0.0 all-gather.2.cloned.1.call-start
  26.2 0.1 copy.35
  26.2 0.1 eq.29
  26.3 0.1 fusion.22
  26.4 0.1 reduce_window_sum.11
  26.6 0.2 select_reduce_fusion
  26.7 0.1 reduce_sum.70
  26.8 0.1 copy.37
  26.9 0.1 convert_reduce_fusion
  27.0 19.7 %all-reduce.2.cloned.1.call-done = bf16[16,2048]{1,0:T(8,128)(2,1)} async-done(((bf16[16,2048]{1,0:T(8,128)(2,1)}), bf16[16,2048]{1,0:T(8,128)(2,1)}) %all-reduce.2.cloned.1.call-update) | async-done | bytes 65552 | tf_op jit(solution)/shard_map/psum | solution.py:61
  46.8 1.6 %convert_add_fusion = (f32[16,2048]{1,0:T(8,128)}, f32[16]{0:T(128)S(1)}) fusion(bf16[16,2048]{1,0:T(8,128)(2,1)S(1)} %copy-done.3, bf16[16,2048]{1,0:T(8,128)(2,1)} %all-reduce.2.cloned.1.call-done), kind=kLoop, calls=%fused_computation.24 | loop fusion | flops 163824 | bytes 262208 | tf_op jit(solution)/shard_map/add | solution.py:62
  48.4 0.9 multiply_convert_fusion
  49.3 0.3 convolution_convert_fusion.3
  49.6 22.2 %all_to_all.21 = bf16[16,16,1024]{2,1,0:T(8,128)(2,1)} all-to-all(bf16[16,16,1024]{2,1,0:T(8,128)(2,1)S(1)} %bitcast.66), channel_id=1, replica_groups=mesh['ep'=16,'tp'=2] {'ep'}, dimensions={0} | all-to-all | bytes 1048576 | tf_op jit(solution)/shard_map/all_to_all | solution.py:98
  71.9 0.2 reduce-scatter.3.cloned.1.call-start
  72.1 7.3 %all-gather.2.cloned.1.call-done = bf16[1,256,2048]{2,1,0:T(8,128)(2,1)} async-done(((bf16[1,256,1024]{2,1,0:T(8,128)(2,1)}), bf16[1,256,2048]{2,1,0:T(8,128)(2,1)}) %all-gather.2.cloned.1.call-update) | async-done | bytes 1048592 | tf_op jit(solution)/shard_map/all_gather | solution.py:99
  79.4 2.1 %fusion.5 = f32[256,256]{1,0:T(8,128)S(1)} fusion(bf16[1,2048,256]{2,1,0:T(8,128)(2,1)} %param.32, bf16[1,256,2048]{2,1,0:T(8,128)(2,1)} %all-gather.2.cloned.1.call-done), kind=kOutput, calls=%fused_computation.13 | convolution fusion | flops 268435456 | bytes 2359296 | tf_op jit(solution)/shard_map/esd,edf->esf/dot_general | solution.py:100
  81.5 3.8 %fusion = bf16[1,256,2048]{2,1,0:T(8,128)(2,1)} fusion(bf16[1,256,2048]{2,1,0:T(8,128)(2,1)} %param.34, bf16[1,2048,256]{2,1,0:T(8,128)(2,1)} %param.33, bf16[1,256,2048]{2,1,0:T(8,128)(2,1)S(1)} %copy-done.2, f32[256,256]{1,0:T(8,128)S(1)} %fusion.5), kind=kOutput, calls=%fused_computation.3 | convolution fusion | flops 537788416 | bytes 4456448 | tf_op jit(solution)/shard_map/esf,efd->esd/dot_general | solution.py:103
  85.4 0.1 mul.203
  85.5 9.6 %reduce-scatter.3.cloned.1.call-done = bf16[1,256,1024]{2,1,0:T(8,128)(2,1)} async-done(((bf16[1,256,2048]{2,1,0:T(8,128)(2,1)}), bf16[1,256,1024]{2,1,0:T(8,128)(2,1)}) %reduce-scatter.3.cloned.1.call-update) | async-done | bytes 524304 | tf_op jit(solution)/shard_map/reduce_scatter | solution.py:106
  95.1 1.9 %copy.51 = bf16[1,256,1024]{2,0,1:T(2,128)(2,1)S(1)} copy(bf16[1,256,1024]{2,1,0:T(8,128)(2,1)} %reduce-scatter.3.cloned.1.call-done) | data formatting | bytes 1048576 | tf_op jit(solution)/shard_map/reduce_scatter | solution.py:106
  96.9 0.5 broadcast.158
  97.4 4.5 %reduce = bf16[256,1024]{1,0:T(8,128)(2,1)} reduce(bf16[256,1,1024]{2,1,0:T(2,128)(2,1)S(1)} %bitcast.64, bf16[]{:T(256)} %broadcast.158), dimensions={1}, to_apply=%bitcast.55.reduce_sub_computation | reduce | bytes 1048578
  101.9 2.2 %reshape.191 = bf16[16,2,8192]{2,1,0:T(2,128)(2,1)} reshape(bf16[256,1024]{1,0:T(8,128)(2,1)} %reduce) | data formatting | bytes 1048576
  104.1 6.8 %all-to-all-start.1 = ((bf16[16,2,8192]{2,1,0:T(2,128)(2,1)}), bf16[16,2,8192]{2,1,0:T(2,128)(2,1)S(1)}, u32[]{:S(2)}, u32[]{:S(2)}) async-start(bf16[16,2,8192]{2,1,0:T(2,128)(2,1)} %reshape.191), calls=%async_computation.2 | async-start | bytes 1048576 | tf_op jit(solution)/shard_map/all_to_all | solution.py:109
  110.9 0.0 reduce-scatter.5.cloned.1.call-start
  111.0 0.1 copy.39
  111.1 1.5 %fusion.51 = f32[16,256]{1,0:T(8,128)S(1)} fusion(bf16[16,2048]{1,0:T(8,128)(2,1)S(1)} %multiply_convert_fusion, bf16[2048,256]{1,0:T(8,128)(2,1)} %param.35), kind=kOutput, calls=%fused_computation.78 | convolution fusion | flops 16777216 | bytes 1130496 | tf_op jit(solution)/shard_map/dot_general | solution.py:68
  112.6 2.9 %convolution_convert_fusion.1 = bf16[16,2048]{1,0:T(8,128)(2,1)} fusion(bf16[256,2048]{1,0:T(8,128)(2,1)} %param.37, bf16[16,2048]{1,0:T(8,128)(2,1)S(1)} %multiply_convert_fusion, bf16[2048,256]{1,0:T(8,128)(2,1)} %param.36, f32[16,256]{1,0:T(8,128)S(1)} %fusion.51), kind=kOutput, calls=%fused_computation.4 | convolution fusion | flops 33611776 | bytes 2244608 | tf_op jit(solution)/shard_map/dot_general | solution.py:71
  115.5 10.9 %all-to-all-done.1 = bf16[16,2,8192]{2,1,0:T(2,128)(2,1)S(1)} async-done(((bf16[16,2,8192]{2,1,0:T(2,128)(2,1)}), bf16[16,2,8192]{2,1,0:T(2,128)(2,1)S(1)}, u32[]{:S(2)}, u32[]{:S(2)}) %all-to-all-start.1) | async-done | bytes 524320 | tf_op jit(solution)/shard_map/all_to_all | solution.py:109
  126.4 1.8 %reshape.192 = bf16[256,1,1024]{2,1,0:T(2,128)(2,1)} reshape(bf16[16,2,8192]{2,1,0:T(2,128)(2,1)S(1)} %all-to-all-done.1) | data formatting | bytes 1048576
  128.2 1.4 %copy.50 = bf16[1,256,1024]{2,1,0:T(8,128)(2,1)S(1)} copy(bf16[1,256,1024]{2,0,1:T(2,128)(2,1)} %bitcast.63) | data formatting | bytes 1048576
  129.6 0.8 gather_fusion
  130.4 0.1 reshape.179
  130.5 0.2 multiply_reduce_fusion
  130.7 0.0 reduce-scatter.5.cloned.1.call-done
  130.8 1.4 %add_convert_fusion = bf16[16,1024]{1,0:T(8,128)(2,1)} fusion(bf16[16,1024]{1,0:T(8,128)(2,1)} %reduce-scatter.5.cloned.1.call-done, f32[16,1024]{1,0:T(8,128)S(1)} %multiply_reduce_fusion, f32[16,2048]{1,0:T(8,128)S(1)} %copy-done.4, s32[]{:T(128)S(6)} %select_n.14), kind=kLoop, calls=%fused_computation.35 | loop fusion | flops 65536 | bytes 196612 | tf_op jit(solution)/shard_map/convert_element_type | solution.py:116
  (43 shorter events, 0.3 us)
Async XLA Ops:
  7.2 17.9 %copy-start = (bf16[512,2048]{1,0:T(8,128)(2,1)S(1)}, bf16[512,2048]{1,0:T(8,128)(2,1)}, u32[]{:S(2)}) copy-start(bf16[512,2048]{1,0:T(8,128)(2,1)} %param.29) | copy-start | bytes 6291460
  7.2 3.3 %copy-start.3 = (bf16[16,2048]{1,0:T(8,128)(2,1)S(1)}, bf16[16,2048]{1,0:T(8,128)(2,1)}, u32[]{:S(2)}) copy-start(bf16[16,2048]{1,0:T(8,128)(2,1)} %param.19) | copy-start | bytes 196612
  7.2 3.3 %copy-start.5 = (f32[2048]{0:T(1024)S(1)}, f32[2048]{0:T(1024)}, u32[]{:S(2)}) copy-start(f32[2048]{0:T(1024)} %param.21) | copy-start | bytes 24580
  7.2 39.6 %all-reduce.2.cloned.1.call-start = ((), (), s32[]{:S(2)}) async-start(), calls=%async_computation.4 | async-start | bytes 131072 | tf_op jit(solution)/shard_map/psum | solution.py:61
  10.5 4.1 %copy-start.8 = (f32[512]{0:T(512)S(1)}, f32[512]{0:T(512)}, u32[]{:S(2)}) copy-start(f32[512]{0:T(512)} %param.28) | copy-start | bytes 6148
  21.1 3.7 %copy-start.1 = (f32[16,4,128,128]{3,2,1,0:T(8,128)}, f32[16,4,128,128]{3,2,1,0:T(8,128)S(1)}, u32[]{:S(2)}) copy-start(f32[16,4,128,128]{3,2,1,0:T(8,128)S(1)} %multiply_add_fusion) | copy-start | bytes 12582916
  21.2 3.8 %copy-start.10 = (f32[128]{0:T(128)S(1)}, f32[128]{0:T(128)}, u32[]{:S(2)}) copy-start(f32[128]{0:T(128)} %param.23) | copy-start | bytes 1540
  24.8 1.3 copy-start.9
  24.8 23.5 %copy-start.7 = (f32[2048]{0:T(1024)S(1)}, f32[2048]{0:T(1024)}, u32[]{:S(2)}) copy-start(f32[2048]{0:T(1024)} %param.22) | copy-start | bytes 24580
  26.1 53.3 %all-gather.2.cloned.1.call-start = ((), (), s32[]{:S(2)}) async-start(), calls=%async_computation.5 | async-start | bytes 1572864 | tf_op jit(solution)/shard_map/all_gather | solution.py:99
  71.9 23.2 %reduce-scatter.3.cloned.1.call-start = ((), (), s32[]{:S(2)}) async-start(), calls=%async_computation.6 | async-start | bytes 1572864 | tf_op jit(solution)/shard_map/reduce_scatter | solution.py:106
  79.4 2.1 %copy-start.2 = (bf16[1,256,2048]{2,1,0:T(8,128)(2,1)S(1)}, bf16[1,256,2048]{2,1,0:T(8,128)(2,1)}, u32[]{:S(2)}) copy-start(bf16[1,256,2048]{2,1,0:T(8,128)(2,1)} %all-gather.2.cloned.1.call-done) | copy-start | bytes 3145732
  81.5 3.9 %copy-start.6 = (f32[16,6]{0,1:T(8,128)S(1)}, f32[16,6]{0,1:T(8,128)}, u32[]{:S(2)}) copy-start(f32[16,6]{0,1:T(8,128)} %param.31) | copy-start | bytes 1156
  104.1 22.3 %all-to-all-start.1 = ((bf16[16,2,8192]{2,1,0:T(2,128)(2,1)}), bf16[16,2,8192]{2,1,0:T(2,128)(2,1)S(1)}, u32[]{:S(2)}, u32[]{:S(2)}) async-start(bf16[16,2,8192]{2,1,0:T(2,128)(2,1)} %reshape.191), calls=%async_computation.2 | async-start | bytes 1048576 | tf_op jit(solution)/shard_map/all_to_all | solution.py:109
  110.9 19.8 %reduce-scatter.5.cloned.1.call-start = ((), (), s32[]{:S(2)}) async-start(), calls=%async_computation.7 | async-start | bytes 98304 | tf_op jit(solution)/shard_map/reduce_scatter | solution.py:72
  128.2 2.5 %copy-start.4 = (f32[16,2048]{1,0:T(8,128)S(1)}, f32[16,2048]{1,0:T(8,128)}, u32[]{:S(2)}) copy-start(f32[16,2048]{1,0:T(8,128)} %get-tuple-element.2) | copy-start | bytes 393220
Sparse Core Ops, SparseCore 0:
  26.2 20.4 all-reduce.1
  72.0 7.3 all-gather.1
  85.5 9.5 reduce-scatter.2
  115.6 8.8 reduce-scatter.4
where the time goes:
time: 140 us; the launch traced here: 139 us
  waiting for transfers between devices  47.6 us (34%)
  matrix products  23.4 us (17%)
  blocking collectives  22.2 us (16%)
  other arithmetic  14.9 us (11%)
  between operations  14.1 us (10%)
  local copies, waits for them, and re-layouts  9.27 us (7%)
  starting transfers between devices  7.14 us (5%)
    all_to_all x1, blocking collectives, local(): lax.all_to_all(outgoing, 'ep', split_axis=0, concat_axis=1, tiled=True)  22.2 us
    psum x1, waiting for transfers between devices, local(): mixer_out = lax.psum(partial_value.astype(jnp.bfloat16), 'tp')  19.7 us
    all_to_all x1, waiting for transfers between devices, local(): lax.all_to_all(expert_half, 'ep', split_axis=1, concat_axis=0, tiled=True)  10.9 us
    reduce_scatter x1, waiting for transfers between devices, local(): lax.psum_scatter(expert_part.astype(jnp.bfloat16), 'tp', scatter_dimensio...  9.58 us
    all_gather x1, waiting for transfers between devices, local(): arrived = lax.all_gather(arrived_half, 'tp', axis=2, tiled=True)  7.3 us
    all_to_all x1, starting transfers between devices, local(): lax.all_to_all(expert_half, 'ep', split_axis=1, concat_axis=0, tiled=True)  6.79 us
    unnamed x29, local copies, waits for them, and re-layouts  6.09 us
    unnamed x1, other arithmetic  4.5 us
  transfers between devices with their start and end apart: 5, of which 4 were waited for; matrix products, arithmetic and copies ran while one was open for 7% of the time, Pallas kernels for 0%

commit v1 on v0

--- a/solution.py
+++ b/solution.py
@@ -58,7 +58,7 @@
     gated_out = (rms_scale(readout, head_gain) * jax.nn.silu(gate_pre)).astype(jnp.bfloat16)
     gated_out = gated_out.reshape(seqs_here, heads_here * value_width)
     partial_value = jnp.dot(gated_out, w_mix_out, preferred_element_type=jnp.float32)
-    mixer_out = lax.psum(partial_value.astype(jnp.bfloat16), "tp")
+    mixer_out = jnp.sum(lax.all_gather(partial_value.astype(jnp.bfloat16), "tp"), axis=0)
     residual = tokens_wide + mixer_out.astype(jnp.float32)
     moe_rows = rms_scale(residual, moe_gain).astype(jnp.bfloat16)
     full_width = moe_rows.shape[1]

time: 140 us -> 121 us (0.86)
  waiting for transfers between devices: 47.6 us -> 27.8 us
  blocking collectives: 22.2 us -> 25.5 us
  other arithmetic: 14.9 us -> 13.3 us
    psum x1 -> x0, waiting for transfers between devices: 19.7 us -> none  [local(): mixer_out = lax.psum(partial_value.astype(jnp.bfloat16), 'tp')]
    all_gather x0 -> x1, blocking collectives: none -> 2.03 us  [local(): lax.all_gather(partial_value.astype(jnp.bfloat16), 'tp')]
  transfers between devices with their start and end apart: 5 -> 4, of which waited for: 4 -> 3; matrix products, arithmetic and copies ran while one was open for 7% -> 7% of each run, Pallas kernels for 0% -> 0%
where the time goes in v1:
time: 121 us; the launch traced here: 120 us
  waiting for transfers between devices  27.8 us (23%)
  blocking collectives  25.5 us (21%)
  matrix products  22.8 us (19%)
  between operations  14.1 us (12%)
  other arithmetic  13.3 us (11%)
  local copies, waits for them, and re-layouts  9.27 us (8%)
  starting transfers between devices  7.23 us (6%)
    all_to_all x1, blocking collectives, local(): lax.all_to_all(outgoing, 'ep', split_axis=0, concat_axis=1, tiled=True)  23.5 us
    all_to_all x1, waiting for transfers between devices, local(): lax.all_to_all(expert_half, 'ep', split_axis=1, concat_axis=0, tiled=True)  10.8 us
    reduce_scatter x1, waiting for transfers between devices, local(): lax.psum_scatter(expert_part.astype(jnp.bfloat16), 'tp', scatter_dimensio...  9.7 us
    all_gather x1, waiting for transfers between devices, local(): arrived = lax.all_gather(arrived_half, 'tp', axis=2, tiled=True)  7.28 us
    all_to_all x1, starting transfers between devices, local(): lax.all_to_all(expert_half, 'ep', split_axis=1, concat_axis=0, tiled=True)  6.92 us
    unnamed x29, local copies, waits for them, and re-layouts  6.09 us
    unnamed x1, other arithmetic  4.5 us
    add x1, other arithmetic, local(): forget[..., None] * state + key_gate[..., None] * input_val[:, :, None, :]  4.39 us
  transfers between devices with their start and end apart: 4, of which 3 were waited for; matrix products, arithmetic and copies ran while one was open for 7% of the time, Pallas kernels for 0%

profile of v1, /device:TPU:0, one launch (start us, length us, event | category | flops | bytes accessed | tf_op | source)
XLA Modules:
  0.0 120.0 jit_solution(10027260449461363775)
XLA Ops:
  7.2 0.0 all-gather.3.cloned.1.call-start
  7.3 1.1 fusion.18
  8.4 2.1 %fusion.40 = f32[16,512]{1,0:T(8,128)S(1)} fusion(bf16[2048,512]{1,0:T(8,128)(2,1)} %param.27, bf16[16,2048]{1,0:T(8,128)(2,1)} %param.19, f32[2048]{0:T(1024)} %param.21, f32[16]{0:T(128)S(1)} %add_rsqrt_fusion.2), kind=kOutput, calls=%fused_computation.72 | convolution fusion | flops 33685504 | bytes 2203712 | tf_op jit(solution)/shard_map/dot_general | solution.py:50
  10.5 2.0 %fusion.44 = f32[16,512]{1,0:T(8,128)S(1)} fusion(bf16[2048,512]{1,0:T(8,128)(2,1)} %param.26, bf16[16,2048]{1,0:T(8,128)(2,1)S(1)} %copy-done.3, f32[2048]{0:T(1024)S(1)} %copy-done.5, f32[16]{0:T(128)S(1)} %add_rsqrt_fusion.2), kind=kOutput, calls=%fused_computation.74 | convolution fusion | flops 33685504 | bytes 2203712 | tf_op jit(solution)/shard_map/dot_general | solution.py:47
  12.5 2.0 %add_divide_fusion.1 = (f32[16,512]{1,0:T(8,128)S(1)}, f32[16,512]{1,0:T(8,128)S(1)}) fusion(bf16[2048,512]{1,0:T(8,128)(2,1)} %param.24, bf16[16,2048]{1,0:T(8,128)(2,1)S(1)} %copy-done.3, f32[2048]{0:T(1024)S(1)} %copy-done.5, f32[16]{0:T(128)S(1)} %add_rsqrt_fusion.2), kind=kOutput, calls=%fused_computation.46 | convolution fusion | flops 33726464 | bytes 2236480 | tf_op jit(solution)/shard_map/dot_general | solution.py:41
  14.6 2.0 %divide_multiply_fusion.1 = f32[16,512]{1,0:T(8,128)S(1)} fusion(bf16[2048,512]{1,0:T(8,128)(2,1)} %param.25, bf16[16,2048]{1,0:T(8,128)(2,1)S(1)} %copy-done.3, f32[2048]{0:T(1024)S(1)} %copy-done.5, f32[16]{0:T(128)S(1)} %add_rsqrt_fusion.2), kind=kOutput, calls=%fused_computation.43 | convolution fusion | flops 33718272 | bytes 2203712 | tf_op jit(solution)/shard_map/dot_general | solution.py:44
  16.7 4.4 %multiply_add_fusion = f32[16,4,128,128]{3,2,1,0:T(8,128)S(1)} fusion(f32[16,4,128,128]{3,2,1,0:T(8,128)} %param.20, f32[16,4,128]{2,1,0:T(4,128)S(1)} %mul.181, f32[16,4,128]{2,1,0:T(4,128)S(1)} %bitcast.72, f32[16,4,128]{2,1,0:T(4,128)S(1)} %bitcast.71), kind=kLoop, calls=%fused_computation.1 | loop fusion | flops 3145728 | bytes 8486912 | tf_op jit(solution)/shard_map/add | solution.py:56
  21.2 3.7 %fusion.50 = f32[16,4,1,128]{3,2,1,0:T(1,128)S(1)} fusion(f32[16,4,128,128]{3,2,1,0:T(8,128)S(1)} %multiply_add_fusion, f32[16,4,128,1]{2,3,1,0:T(1,128)S(1)} %bitcast.73), kind=kOutput, calls=%fused_computation.77 | convolution fusion | flops 12582912 | bytes 4259840 | tf_op jit(solution)/shard_map/shkv,shk->shv/dot_general | solution.py:57
  24.8 0.1 multiply_reduce_fusion.2
  25.0 0.1 fusion.25
  25.1 0.4 convolution_convert_fusion.2
  25.5 2.0 %all-gather = bf16[32,2048]{1,0:T(8,128)(2,1)S(1)} all-gather(bf16[16,2048]{1,0:T(8,128)(2,1)S(1)} %convolution_convert_fusion.2), channel_id=2, replica_groups=mesh['ep'=16,'tp'=2] {'tp'}, dimensions={0}, use_global_device_ids=true | all-gather | bytes 196608 | tf_op jit(solution)/shard_map/all_gather | solution.py:61
  27.5 0.8 convert_add_fusion
  28.3 0.1 copy.35
  28.4 0.1 eq.29
  28.5 0.1 fusion.22
  28.6 0.1 reduce_window_sum.11
  28.7 0.2 select_reduce_fusion
  28.9 0.1 reduce_sum.83
  29.0 0.1 copy.37
  29.1 0.1 convert_reduce_fusion
  29.2 0.1 multiply_convert_fusion
  29.3 0.3 convolution_convert_fusion.3
  29.6 23.5 %all_to_all.21 = bf16[16,16,1024]{2,1,0:T(8,128)(2,1)} all-to-all(bf16[16,16,1024]{2,1,0:T(8,128)(2,1)S(1)} %bitcast.67), channel_id=1, replica_groups=mesh['ep'=16,'tp'=2] {'ep'}, dimensions={0} | all-to-all | bytes 1048576 | tf_op jit(solution)/shard_map/all_to_all | solution.py:98
  53.1 0.0 all-gather.3.cloned.1.call-update
  53.1 0.2 reduce-scatter.3.cloned.1.call-start
  53.4 7.3 %all-gather.3.cloned.1.call-done = bf16[1,256,2048]{2,1,0:T(8,128)(2,1)} async-done(((bf16[1,256,1024]{2,1,0:T(8,128)(2,1)}), bf16[1,256,2048]{2,1,0:T(8,128)(2,1)}) %all-gather.3.cloned.1.call-update) | async-done | bytes 1048592 | tf_op jit(solution)/shard_map/all_gather | solution.py:99
  60.6 2.1 %fusion.5 = f32[256,256]{1,0:T(8,128)S(1)} fusion(bf16[1,2048,256]{2,1,0:T(8,128)(2,1)} %param.32, bf16[1,256,2048]{2,1,0:T(8,128)(2,1)} %all-gather.3.cloned.1.call-done), kind=kOutput, calls=%fused_computation.13 | convolution fusion | flops 268435456 | bytes 2359296 | tf_op jit(solution)/shard_map/esd,edf->esf/dot_general | solution.py:100
  62.7 3.8 %fusion = bf16[1,256,2048]{2,1,0:T(8,128)(2,1)} fusion(bf16[1,256,2048]{2,1,0:T(8,128)(2,1)} %param.34, bf16[1,2048,256]{2,1,0:T(8,128)(2,1)} %param.33, bf16[1,256,2048]{2,1,0:T(8,128)(2,1)S(1)} %copy-done.2, f32[256,256]{1,0:T(8,128)S(1)} %fusion.5), kind=kOutput, calls=%fused_computation.3 | convolution fusion | flops 537788416 | bytes 4456448 | tf_op jit(solution)/shard_map/esf,efd->esd/dot_general | solution.py:103
  66.6 9.7 %reduce-scatter.3.cloned.1.call-done = bf16[1,256,1024]{2,1,0:T(8,128)(2,1)} async-done(((bf16[1,256,2048]{2,1,0:T(8,128)(2,1)}), bf16[1,256,1024]{2,1,0:T(8,128)(2,1)}) %reduce-scatter.3.cloned.1.call-update) | async-done | bytes 524304 | tf_op jit(solution)/shard_map/reduce_scatter | solution.py:106
  76.3 1.9 %copy.51 = bf16[1,256,1024]{2,0,1:T(2,128)(2,1)S(1)} copy(bf16[1,256,1024]{2,1,0:T(8,128)(2,1)} %reduce-scatter.3.cloned.1.call-done) | data formatting | bytes 1048576 | tf_op jit(solution)/shard_map/reduce_scatter | solution.py:106
  78.1 0.5 broadcast.158
  78.6 4.5 %reduce.1 = bf16[256,1024]{1,0:T(8,128)(2,1)} reduce(bf16[256,1,1024]{2,1,0:T(2,128)(2,1)S(1)} %bitcast.65, bf16[]{:T(256)} %broadcast.158), dimensions={1}, to_apply=%bitcast.56.reduce_sub_computation | reduce | bytes 1048578
  83.1 2.2 %reshape.192 = bf16[16,2,8192]{2,1,0:T(2,128)(2,1)} reshape(bf16[256,1024]{1,0:T(8,128)(2,1)} %reduce.1) | data formatting | bytes 1048576
  85.4 6.9 %all-to-all-start.1 = ((bf16[16,2,8192]{2,1,0:T(2,128)(2,1)}), bf16[16,2,8192]{2,1,0:T(2,128)(2,1)S(1)}, u32[]{:S(2)}, u32[]{:S(2)}) async-start(bf16[16,2,8192]{2,1,0:T(2,128)(2,1)} %reshape.192), calls=%async_computation.2 | async-start | bytes 1048576 | tf_op jit(solution)/shard_map/all_to_all | solution.py:109
  92.3 0.0 reduce-scatter.5.cloned.1.call-start
  92.3 1.5 %fusion.51 = f32[16,256]{1,0:T(8,128)S(1)} fusion(bf16[16,2048]{1,0:T(8,128)(2,1)S(1)} %multiply_convert_fusion, bf16[2048,256]{1,0:T(8,128)(2,1)} %param.35), kind=kOutput, calls=%fused_computation.78 | convolution fusion | flops 16777216 | bytes 1130496 | tf_op jit(solution)/shard_map/dot_general | solution.py:68
  93.8 2.9 %convolution_convert_fusion.1 = bf16[16,2048]{1,0:T(8,128)(2,1)} fusion(bf16[256,2048]{1,0:T(8,128)(2,1)} %param.37, bf16[16,2048]{1,0:T(8,128)(2,1)S(1)} %multiply_convert_fusion, bf16[2048,256]{1,0:T(8,128)(2,1)} %param.36, f32[16,256]{1,0:T(8,128)S(1)} %fusion.51), kind=kOutput, calls=%fused_computation.4 | convolution fusion | flops 33611776 | bytes 2244608 | tf_op jit(solution)/shard_map/dot_general | solution.py:71
  96.7 0.1 mul.203
  96.9 0.1 copy.39
  97.0 10.8 %all-to-all-done.1 = bf16[16,2,8192]{2,1,0:T(2,128)(2,1)S(1)} async-done(((bf16[16,2,8192]{2,1,0:T(2,128)(2,1)}), bf16[16,2,8192]{2,1,0:T(2,128)(2,1)S(1)}, u32[]{:S(2)}, u32[]{:S(2)}) %all-to-all-start.1) | async-done | bytes 524320 | tf_op jit(solution)/shard_map/all_to_all | solution.py:109
  107.8 1.8 %reshape.193 = bf16[256,1,1024]{2,1,0:T(2,128)(2,1)} reshape(bf16[16,2,8192]{2,1,0:T(2,128)(2,1)S(1)} %all-to-all-done.1) | data formatting | bytes 1048576
  109.6 1.4 %copy.50 = bf16[1,256,1024]{2,1,0:T(8,128)(2,1)S(1)} copy(bf16[1,256,1024]{2,0,1:T(2,128)(2,1)} %bitcast.64) | data formatting | bytes 1048576
  111.0 0.8 gather_fusion
  111.8 0.1 reshape.179
  111.8 0.2 multiply_reduce_fusion
  112.1 0.0 reduce-scatter.5.cloned.1.call-done
  112.1 1.4 %add_convert_fusion = bf16[16,1024]{1,0:T(8,128)(2,1)} fusion(bf16[16,1024]{1,0:T(8,128)(2,1)} %reduce-scatter.5.cloned.1.call-done, f32[16,1024]{1,0:T(8,128)S(1)} %multiply_reduce_fusion, f32[16,2048]{1,0:T(8,128)S(1)} %copy-done.4, s32[]{:T(128)S(6)} %select_n.14), kind=kLoop, calls=%fused_computation.35 | loop fusion | flops 65536 | bytes 196612 | tf_op jit(solution)/shard_map/convert_element_type | solution.py:116
  (42 shorter events, 0.3 us)
Async XLA Ops:
  7.2 17.9 %copy-start = (bf16[512,2048]{1,0:T(8,128)(2,1)S(1)}, bf16[512,2048]{1,0:T(8,128)(2,1)}, u32[]{:S(2)}) copy-start(bf16[512,2048]{1,0:T(8,128)(2,1)} %param.29) | copy-start | bytes 6291460
  7.2 3.3 %copy-start.3 = (bf16[16,2048]{1,0:T(8,128)(2,1)S(1)}, bf16[16,2048]{1,0:T(8,128)(2,1)}, u32[]{:S(2)}) copy-start(bf16[16,2048]{1,0:T(8,128)(2,1)} %param.19) | copy-start | bytes 196612
  7.2 3.3 %copy-start.5 = (f32[2048]{0:T(1024)S(1)}, f32[2048]{0:T(1024)}, u32[]{:S(2)}) copy-start(f32[2048]{0:T(1024)} %param.21) | copy-start | bytes 24580
  7.2 53.4 %all-gather.3.cloned.1.call-start = ((), (), s32[]{:S(2)}) async-start(), calls=%async_computation.4 | async-start | bytes 1572864 | tf_op jit(solution)/shard_map/all_gather | solution.py:99
  10.5 4.1 %copy-start.8 = (f32[512]{0:T(512)S(1)}, f32[512]{0:T(512)}, u32[]{:S(2)}) copy-start(f32[512]{0:T(512)} %param.28) | copy-start | bytes 6148
  21.1 3.7 %copy-start.1 = (f32[16,4,128,128]{3,2,1,0:T(8,128)}, f32[16,4,128,128]{3,2,1,0:T(8,128)S(1)}, u32[]{:S(2)}) copy-start(f32[16,4,128,128]{3,2,1,0:T(8,128)S(1)} %multiply_add_fusion) | copy-start | bytes 12582916
  21.2 3.8 %copy-start.10 = (f32[128]{0:T(128)S(1)}, f32[128]{0:T(128)}, u32[]{:S(2)}) copy-start(f32[128]{0:T(128)} %param.23) | copy-start | bytes 1540
  24.8 3.5 %copy-start.9 = (s32[16,6]{0,1:T(8,128)S(1)}, s32[16,6]{0,1:T(8,128)}, u32[]{:S(2)}) copy-start(s32[16,6]{0,1:T(8,128)} %param.30) | copy-start | bytes 1156
  24.8 4.3 %copy-start.7 = (f32[2048]{0:T(1024)S(1)}, f32[2048]{0:T(1024)}, u32[]{:S(2)}) copy-start(f32[2048]{0:T(1024)} %param.22) | copy-start | bytes 24580
  53.1 23.1 %reduce-scatter.3.cloned.1.call-start = ((), (), s32[]{:S(2)}) async-start(), calls=%async_computation.5 | async-start | bytes 1572864 | tf_op jit(solution)/shard_map/reduce_scatter | solution.py:106
  60.6 2.1 %copy-start.2 = (bf16[1,256,2048]{2,1,0:T(8,128)(2,1)S(1)}, bf16[1,256,2048]{2,1,0:T(8,128)(2,1)}, u32[]{:S(2)}) copy-start(bf16[1,256,2048]{2,1,0:T(8,128)(2,1)} %all-gather.3.cloned.1.call-done) | copy-start | bytes 3145732
  85.4 11.5 %copy-start.6 = (f32[16,6]{0,1:T(8,128)S(1)}, f32[16,6]{0,1:T(8,128)}, u32[]{:S(2)}) copy-start(f32[16,6]{0,1:T(8,128)} %param.31) | copy-start | bytes 1156
  85.4 22.4 %all-to-all-start.1 = ((bf16[16,2,8192]{2,1,0:T(2,128)(2,1)}), bf16[16,2,8192]{2,1,0:T(2,128)(2,1)S(1)}, u32[]{:S(2)}, u32[]{:S(2)}) async-start(bf16[16,2,8192]{2,1,0:T(2,128)(2,1)} %reshape.192), calls=%async_computation.2 | async-start | bytes 1048576 | tf_op jit(solution)/shard_map/all_to_all | solution.py:109
  92.3 19.8 %reduce-scatter.5.cloned.1.call-start = ((), (), s32[]{:S(2)}) async-start(), calls=%async_computation.6 | async-start | bytes 98304 | tf_op jit(solution)/shard_map/reduce_scatter | solution.py:72
  109.6 2.5 %copy-start.4 = (f32[16,2048]{1,0:T(8,128)S(1)}, f32[16,2048]{1,0:T(8,128)}, u32[]{:S(2)}) copy-start(f32[16,2048]{1,0:T(8,128)} %get-tuple-element.2) | copy-start | bytes 393220
Sparse Core Ops, SparseCore 0:
  53.2 7.3 all-gather.2
  66.7 9.5 reduce-scatter.2
  96.9 8.8 reduce-scatter.4
